TPU v7x, 32 devices: a whole 2x2x4 slice. The times are simulated.
32 devices in a mesh: fs: 4 (over z), rep: 4 (over y, x), tp: 2 (over core).
Axes of the slice: x: 2, y: 2, z: 4, core: 2. Of those that a mesh axis runs over, the one named last changes fastest.
Arguments:
- mixer_input: bfloat16 [32768, 2048], P(('fs', 'rep')), may hold values from -6 to 6
- value_cot: bfloat16 [32768, 2048], P(('fs', 'rep'), 'tp'), may hold values from -0.22097087 to 0.22097087
- gate_cot: bfloat16 [32768, 2048], P(('fs', 'rep'), 'tp'), may hold values from -0.22097087 to 0.22097087
- value_weight: float32 [2048, 2048], P('fs', 'tp'), may hold values from -0.125 to 0.125
- gate_weight: float32 [2048, 2048], P('fs', 'tp'), may hold values from -0.125 to 0.125
- value_basis: bfloat16 [2048, 256], replicated, may hold values from -0.8838835 to 0.8838835
- gate_basis: bfloat16 [2048, 256], replicated, may hold values from -0.8838835 to 0.8838835
- value_first: float32 [256, 2048], P('fs', 'tp'), may hold values from -6 to 6
- gate_first: float32 [256, 2048], P('fs', 'tp'), may hold values from -6 to 6
- value_second: float32 [256, 2048], P('fs', 'tp'), may hold values from 0.01 to 1
- gate_second: float32 [256, 2048], P('fs', 'tp'), may hold values from 0.01 to 1
Outputs:
- value_new: float32 [2048, 2048], P('fs', 'tp')
- gate_new: float32 [2048, 2048], P('fs', 'tp')
- value_copy: bfloat16 [2048, 2048], P(None, 'tp')
- gate_copy: bfloat16 [2048, 2048], P(None, 'tp')
- value_step: float32 [2048, 2048], P('fs', 'tp')
- gate_step: float32 [2048, 2048], P('fs', 'tp')
- value_first_new: float32 [256, 2048], P('fs', 'tp')
- gate_first_new: float32 [256, 2048], P('fs', 'tp')
- value_second_new: float32 [256, 2048], P('fs', 'tp')
- gate_second_new: float32 [256, 2048], P('fs', 'tp')
All inputs are finite; a program needn't handle non-finite values.
Results may differ from a plain program's by a relative error of at most 0.0044.
Values may be sent and summed in bfloat16 or wider, within the bound.
A program may use at most 128 MiB of HBM per device.

v0:
```python
import jax
import jax.numpy as jnp
from jax import lax
from jax.sharding import PartitionSpec as P

D = 2048


learn_rate = 0.02


def local(
    mixer_input,
    value_cot,
    gate_cot,
    value_weight,
    gate_weight,
    value_basis,
    gate_basis,
    value_first,
    gate_first,
    value_second,
    gate_second,
):
    half_cols = value_cot.shape[1]
    rows_dev = value_weight.shape[0]
    fs_index = lax.axis_index("fs")
    own_value = lax.dynamic_slice_in_dim(value_basis, fs_index * rows_dev, rows_dev, 0)
    own_gate = lax.dynamic_slice_in_dim(gate_basis, fs_index * rows_dev, rows_dev, 0)
    value_proj = jnp.dot(mixer_input, value_basis, preferred_element_type=jnp.float32)
    gate_proj = jnp.dot(mixer_input, gate_basis, preferred_element_type=jnp.float32)
    upper_value = lax.optimization_barrier(value_proj.astype(jnp.bfloat16))
    upper_gate = lax.optimization_barrier(gate_proj.astype(jnp.bfloat16))
    lower_value = (value_proj - upper_value.astype(jnp.float32)).astype(jnp.bfloat16)
    lower_gate = (gate_proj - upper_gate.astype(jnp.float32)).astype(jnp.bfloat16)
    value_part = jnp.dot(upper_value.T, value_cot, preferred_element_type=jnp.float32) + jnp.dot(
        lower_value.T, value_cot, preferred_element_type=jnp.float32
    )
    gate_part = jnp.dot(upper_gate.T, gate_cot, preferred_element_type=jnp.float32) + jnp.dot(
        lower_gate.T, gate_cot, preferred_element_type=jnp.float32
    )
    partial_value = lax.psum_scatter(
        jnp.concatenate([value_part, gate_part], axis=1), "fs", scatter_dimension=0, tiled=True
    )
    projected = lax.psum(partial_value, "rep")
    value_small = projected[:, :half_cols]
    gate_small = projected[:, half_cols:]
    value_first_new = 0.9 * value_first + 0.1 * value_small
    gate_first_new = 0.9 * gate_first + 0.1 * gate_small
    value_second_new = 0.95 * value_second + 0.05 * value_small * value_small
    gate_second_new = 0.95 * gate_second + 0.05 * gate_small * gate_small
    scaled = jnp.concatenate(
        [
            value_first_new * lax.rsqrt(value_second_new),
            gate_first_new * lax.rsqrt(gate_second_new),
        ],
        axis=1,
    ).astype(jnp.bfloat16)
    piece = lax.all_gather(scaled, "fs", axis=0, tiled=True)
    value_part = jnp.dot(own_value, piece[:, :half_cols], preferred_element_type=jnp.float32)
    gate_part = jnp.dot(own_gate, piece[:, half_cols:], preferred_element_type=jnp.float32)
    expanded = jnp.concatenate([value_part, gate_part], axis=1)
    value_full = expanded[:, :half_cols]
    gate_full = expanded[:, half_cols:]
    squares = lax.psum(
        (jnp.sum(value_full * value_full), jnp.sum(gate_full * gate_full)), ("fs", "tp")
    )
    entries = float(D * D)
    value_step = value_full * lax.rsqrt(squares[0] / entries + 1e-06)
    gate_step = gate_full * lax.rsqrt(squares[1] / entries + 1e-06)
    value_new = value_weight - learn_rate * value_step
    gate_new = gate_weight - learn_rate * gate_step
    copies = (
        lax.all_gather(value_new.astype(jnp.bfloat16), "fs", axis=0, tiled=True),
        lax.all_gather(gate_new.astype(jnp.bfloat16), "fs", axis=0, tiled=True),
    )
    return (
        value_new,
        gate_new,
        copies[0],
        copies[1],
        value_step,
        gate_step,
        value_first_new,
        gate_first_new,
        value_second_new,
        gate_second_new,
    )


def solution(mesh):
    return jax.shard_map(
        local,
        mesh=mesh,
        in_specs=(
            P(("fs", "rep"), None),
            P(("fs", "rep"), "tp"),
            P(("fs", "rep"), "tp"),
            P("fs", "tp"),
            P("fs", "tp"),
            P(),
            P(),
            P("fs", "tp"),
            P("fs", "tp"),
            P("fs", "tp"),
            P("fs", "tp"),
        ),
        out_specs=(
            P("fs", "tp"),
            P("fs", "tp"),
            P(None, "tp"),
            P(None, "tp"),
            P("fs", "tp"),
            P("fs", "tp"),
            P("fs", "tp"),
            P("fs", "tp"),
            P("fs", "tp"),
            P("fs", "tp"),
        ),
        check_vma=False,
    )
```

profile of v0, /device:TPU:0, one launch (start us, length us, event | category | flops | bytes accessed | tf_op | source)
XLA Modules:
  0.0 350.1 jit_solution(15234940572082400259)
XLA Ops:
  7.2 0.0 reduce-scatter.2.cloned.1.call-start
  7.2 6.2 %fusion.15 = (bf16[2048,256]{1,0:T(8,128)(2,1)S(1)}, f32[2048,256]{1,0:T(8,128)S(1)}) fusion(bf16[2048,2048]{1,0:T(8,128)(2,1)} %param.11, bf16[2048,256]{1,0:T(8,128)(2,1)} %param.16), kind=kOutput, calls=%fused_computation.31 | convolution fusion | flops 2148007936 | bytes 12582912 | tf_op jit(solution)/shard_map/dot_general | solution.py:30
  13.5 0.1 copy-done.9
  13.6 2.4 fusion.14
  16.1 1.3 fusion.16
  17.3 1.3 convolution_add_fusion.1
  18.6 0.9 copy-done.2
  19.5 1.3 fusion.17
  20.8 1.3 convolution_add_fusion
  22.1 1.5 pad_maximum_fusion
  23.6 0.0 reduce-scatter.2.cloned.1.call-update
  23.6 0.0 all-reduce.3.cloned.1.call-start
  23.6 46.5 %reduce-scatter.2.cloned.1.call-done = f32[64,2048]{1,0:T(8,128)} async-done(((f32[256,2048]{1,0:T(8,128)}), f32[64,2048]{1,0:T(8,128)}) %reduce-scatter.2.cloned.1.call-update) | async-done | bytes 524304 | tf_op jit(solution)/shard_map/reduce_scatter | solution.py:42
  70.1 0.0 all-reduce.3.cloned.1.call-update
  70.1 0.0 all-gather.4.cloned.1.call-start
  70.2 47.5 %all-reduce.3.cloned.1.call-done = f32[64,2048]{1,0:T(8,128)} async-done(((f32[64,2048]{1,0:T(8,128)}), f32[64,2048]{1,0:T(8,128)}) %all-reduce.3.cloned.1.call-update) | async-done | bytes 524304 | tf_op jit(solution)/shard_map/psum | solution.py:45
  117.7 2.1 multiply_convert_fusion.1
  119.8 0.7 pad_maximum_fusion.1
  120.5 0.0 all-gather.4.cloned.1.call-update
  120.5 0.0 all-gather.6.cloned.1.call-start
  120.6 28.1 %all-gather.4.cloned.1.call-done = bf16[256,2048]{1,0:T(8,128)(2,1)} async-done(((bf16[64,2048]{1,0:T(8,128)(2,1)}), bf16[256,2048]{1,0:T(8,128)(2,1)}) %all-gather.4.cloned.1.call-update) | async-done | bytes 1048592 | tf_op jit(solution)/shard_map/all_gather | solution.py:59
  148.7 2.4 multiply_reduce_fusion
  151.1 3.5 multiply_reduce_fusion.1
  154.6 15.3 %all-reduce = (f32[]{:T(128)}, f32[]{:T(128)}) all-reduce(f32[]{:T(128)} %get-tuple-element.31, f32[]{:T(128)} %get-tuple-element.33), channel_id=1, replica_groups=mesh['fs'=4,'rep'=4,'tp'=2] {'fs','tp'}, use_global_device_ids=true, to_apply=%region_3.0 | all-reduce | flops 2 | bytes 16 | tf_op jit(solution)/shard_map/psum | solution.py:65
  170.6 5.6 %fusion.11 = (bf16[512,1024]{1,0:T(8,128)(2,1)}, f32[512,1024]{1,0:T(8,128)}, f32[512,1024]{1,0:T(8,128)}) fusion(f32[512,1024]{1,0:T(8,128)} %param.14, f32[512,1024]{1,0:T(8,128)} %get-tuple-element.32, f32[]{:T(128)S(6)} %rsqrt.14), kind=kLoop, calls=%fused_computation.29 | loop fusion | flops 2097152 | bytes 9437188 | tf_op jit(solution)/shard_map/convert_element_type | solution.py:74
  176.2 0.0 all-gather.6.cloned.1.call-update
  176.2 0.0 all-gather.8.cloned.1.call-start
  177.0 4.8 %fusion.10 = (bf16[512,1024]{1,0:T(8,128)(2,1)}, f32[512,1024]{1,0:T(8,128)}, f32[512,1024]{1,0:T(8,128)}) fusion(f32[512,1024]{1,0:T(8,128)} %param.15, f32[512,1024]{1,0:T(8,128)S(1)} %get-tuple-element.34, f32[]{:T(128)S(6)} %rsqrt.15), kind=kLoop, calls=%fused_computation.28 | loop fusion | flops 2097152 | bytes 9437188 | tf_op jit(solution)/shard_map/convert_element_type | solution.py:75
  181.7 73.7 %all-gather.6.cloned.1.call-done = bf16[2048,1024]{1,0:T(8,128)(2,1)} async-done(((bf16[512,1024]{1,0:T(8,128)(2,1)}), bf16[2048,1024]{1,0:T(8,128)(2,1)}) %all-gather.6.cloned.1.call-update) | async-done | bytes 4194320 | tf_op jit(solution)/shard_map/all_gather | solution.py:74
  255.5 81.2 %all-gather.8.cloned.1.call-done = bf16[2048,1024]{1,0:T(8,128)(2,1)} async-done(((bf16[512,1024]{1,0:T(8,128)(2,1)}), bf16[2048,1024]{1,0:T(8,128)(2,1)}) %all-gather.8.cloned.1.call-update) | async-done | bytes 4194320 | tf_op jit(solution)/shard_map/all_gather | solution.py:75
  336.7 4.8 %copy.24 = bf16[2048,1024]{1,0:T(8,128)(2,1)} copy(bf16[2048,1024]{1,0:T(8,128)(2,1)} %all-gather.6.cloned.1.call-done) | data formatting | bytes 8388608
  341.5 2.0 copy.25
  (19 shorter events, 0.1 us)
Async XLA Ops:
  7.2 6.3 %copy-start = (bf16[2048,256]{1,0:T(8,128)(2,1)S(1)}, bf16[2048,256]{1,0:T(8,128)(2,1)}, u32[]{:S(2)}) copy-start(bf16[2048,256]{1,0:T(8,128)(2,1)} %param.17) | copy-start | bytes 3145732
  7.2 62.9 %reduce-scatter.2.cloned.1.call-start = ((), (), s32[]{:S(2)}) async-start(), calls=%async_computation.1 | async-start | bytes 2621440 | tf_op jit(solution)/shard_map/reduce_scatter | solution.py:42
  7.2 6.4 %copy-start.9 = (bf16[2048,2048]{1,0:T(8,128)(2,1)S(1)}, bf16[2048,2048]{1,0:T(8,128)(2,1)}, u32[]{:S(2)}) copy-start(bf16[2048,2048]{1,0:T(8,128)(2,1)} %param.11) | copy-start | bytes 25165828
  13.6 2.4 copy-start.1
  17.3 2.2 copy-start.2
  23.5 94.1 %copy-start.5 = (f32[64,1024]{1,0:T(8,128)S(1)}, f32[64,1024]{1,0:T(8,128)}, u32[]{:S(2)}) copy-start(f32[64,1024]{1,0:T(8,128)} %param.20) | copy-start | bytes 786436
  23.5 94.1 %copy-start.6 = (f32[64,1024]{1,0:T(8,128)S(1)}, f32[64,1024]{1,0:T(8,128)}, u32[]{:S(2)}) copy-start(f32[64,1024]{1,0:T(8,128)} %param.18) | copy-start | bytes 786436
  23.5 94.1 %copy-start.7 = (f32[64,1024]{1,0:T(8,128)S(1)}, f32[64,1024]{1,0:T(8,128)}, u32[]{:S(2)}) copy-start(f32[64,1024]{1,0:T(8,128)} %param.21) | copy-start | bytes 786436
  23.6 94.1 %copy-start.8 = (f32[64,1024]{1,0:T(8,128)S(1)}, f32[64,1024]{1,0:T(8,128)}, u32[]{:S(2)}) copy-start(f32[64,1024]{1,0:T(8,128)} %param.19) | copy-start | bytes 786436
  23.6 94.1 %all-reduce.3.cloned.1.call-start = ((), (), s32[]{:S(2)}) async-start(), calls=%async_computation.2 | async-start | bytes 1048576 | tf_op jit(solution)/shard_map/psum | solution.py:45
  70.1 78.6 %all-gather.4.cloned.1.call-start = ((), (), s32[]{:S(2)}) async-start(), calls=%async_computation.3 | async-start | bytes 1310720 | tf_op jit(solution)/shard_map/all_gather | solution.py:59
  120.5 134.9 %all-gather.6.cloned.1.call-start = ((), (), s32[]{:S(2)}) async-start(), calls=%async_computation.4 | async-start | bytes 5242880 | tf_op jit(solution)/shard_map/all_gather | solution.py:74
  148.7 2.4 copy-start.4
  176.2 160.5 %all-gather.8.cloned.1.call-start = ((), (), s32[]{:S(2)}) async-start(), calls=%async_computation.5 | async-start | bytes 5242880 | tf_op jit(solution)/shard_map/all_gather | solution.py:75
  336.7 4.8 %copy-start.3 = (bf16[2048,1024]{1,0:T(8,128)(2,1)S(1)}, bf16[2048,1024]{1,0:T(8,128)(2,1)}, u32[]{:S(2)}) copy-start(bf16[2048,1024]{1,0:T(8,128)(2,1)} %all-gather.8.cloned.1.call-done) | copy-start | bytes 12582916
Sparse Core Ops, SparseCore 0:
  23.7 46.3 reduce-scatter.1
  73.1 44.5 all-reduce.2
  120.7 27.9 all-gather.3
  176.3 79.0 all-gather.5
  257.5 79.2 all-gather.7
where the time goes:
time: 350 us
  waiting for transfers between devices  277 us (79%)
  matrix products  19.7 us (6%)
  blocking collectives  15.3 us (4%)
  between operations  15.3 us (4%)
  other arithmetic  14.6 us (4%)
  local copies, waits for them, and re-layouts  7.86 us (2%)
    all_gather x1, waiting for transfers between devices, local(): lax.all_gather(gate_new.astype(jnp.bfloat16), 'fs', axis=0, tiled=True)  81.2 us
    all_gather x1, waiting for transfers between devices, local(): lax.all_gather(value_new.astype(jnp.bfloat16), 'fs', axis=0, tiled=True)  73.7 us
    psum x1, waiting for transfers between devices, local(): projected = lax.psum(partial_value, 'rep')  47.5 us
    reduce_scatter x1, waiting for transfers between devices, local(): lax.psum_scatter(jnp.concatenate([value_part, gate_part], axis=1), 'fs',...  46.5 us
    all_gather x1, waiting for transfers between devices, local(): piece = lax.all_gather(scaled, 'fs', axis=0, tiled=True)  28.1 us
    psum x1, blocking collectives, local(): lax.psum((jnp.sum(value_full * value_full), jnp.sum(gate_full * gate_full...  15.3 us
    unnamed x22, local copies, waits for them, and re-layouts  7.86 us
  transfers between devices with their start and end apart: 5, of which 5 were waited for; matrix products, arithmetic and copies ran while one was open for 1% of the time, Pallas kernels for 0%

commit v1 on v0

v1 whole, which is shorter than its diff:
```python
import functools

import jax
import jax.numpy as jnp
from jax import lax
from jax.experimental import pallas as pl
from jax.experimental.pallas import tpu as pltpu
from jax.sharding import PartitionSpec as P

learn_rate = 0.02
CHUNKS = 4
F32 = jnp.float32
BF16 = jnp.bfloat16


def dot(a, b):
    return jnp.dot(a, b, preferred_element_type=F32)


def dot_first(a, b):
    return lax.dot_general(a, b, (((0,), (0,)), ((), ())), preferred_element_type=F32)


def split(a):
    upper = a.astype(BF16)
    return upper, (a - upper.astype(F32)).astype(BF16)


def exchange(
    n_fs, n_rep, n_tp,
    mixer, value_cot, gate_cot, value_weight, gate_weight, value_basis, gate_basis,
    value_first, gate_first, value_second, gate_second,
    value_rows, gate_rows, scaled_out, projected_out, squares_out,
    x_buf, cot_buf, w_buf, w_half, basis_buf, gram, acc, part_in,
    mid, mid_in, proj_all, scaled, sq_buf,
    x_sem, w_sem, b_sem, own_sem,
    w1_send, w1_recv, w2_send, w2_recv,
    s1_send, s1_recv, s2_send, s2_recv, p_send, p_recv, a_send, a_recv, g_send, g_recv, q_send, q_recv,
):
    f, r, t = lax.axis_index("fs"), lax.axis_index("rep"), lax.axis_index("tp")
    cots = (value_cot, gate_cot)
    weights = (value_weight, gate_weight)
    bases = (value_basis, gate_basis)
    gathered = (value_rows, gate_rows)
    tokens = mixer.shape[0]
    chunk = tokens // CHUNKS
    rows = value_weight.shape[0]
    share = rows // n_rep
    width = acc.shape[2]
    per_role = n_rep // 2
    low = mid.shape[1]

    def fs_at(d):
        return lax.rem(f + d, n_fs)

    def rep_at(d):
        return lax.rem(r + d, n_rep)

    def send(src, dst, s, v, **where):
        return pltpu.make_async_remote_copy(
            src_ref=src, dst_ref=dst, send_sem=s, recv_sem=v,
            device_id=where, device_id_type=pl.DeviceIdType.MESH,
        )

    w_loads = [pltpu.make_async_copy(weights[k], w_buf.at[k], w_sem.at[k]) for k in range(2)]
    b_loads = [pltpu.make_async_copy(bases[k], basis_buf.at[k], b_sem.at[k]) for k in range(2)]

    def x_loads(c):
        span = pl.ds(pl.multiple_of(c * chunk, chunk), chunk)
        return [pltpu.make_async_copy(mixer.at[span], x_buf.at[c], x_sem.at[c, 0])] + [
            pltpu.make_async_copy(cots[k].at[span], cot_buf.at[k, c], x_sem.at[c, 1 + k]) for k in range(2)
        ]

    for copy in w_loads + b_loads:
        copy.start()
    for c in range(CHUNKS):
        for copy in x_loads(c):
            copy.start()

    barrier = pltpu.get_barrier_semaphore()
    for d in range(1, n_fs):
        pl.semaphore_signal(barrier, inc=1, device_id={"fs": fs_at(d)}, device_id_type=pl.DeviceIdType.MESH)
    for d in range(1, n_rep):
        pl.semaphore_signal(barrier, inc=1, device_id={"rep": rep_at(d)}, device_id_type=pl.DeviceIdType.MESH)
    for d in range(1, n_tp):
        pl.semaphore_signal(
            barrier, inc=1, device_id={"tp": lax.rem(t + d, n_tp)}, device_id_type=pl.DeviceIdType.MESH
        )
    for k in range(2):
        w_loads[k].wait()
        w_half[k] = w_buf[k].astype(BF16)
    pl.semaphore_wait(barrier, n_fs + n_rep + n_tp - 3)

    def share_of(block, part_index):
        return pl.ds(pl.multiple_of(block * rows + part_index * share, share), share)

    w1 = {}
    for d in range(1, n_fs):
        for k in range(2):
            w1[d, k] = send(
                w_half.at[k, pl.ds(pl.multiple_of(r * share, share), share)],
                gathered[k].at[share_of(f, r)],
                w1_send.at[d - 1, k], w1_recv.at[d - 1, k], fs=fs_at(d),
            )
            w1[d, k].start()
    own = []
    for k in range(2):
        copy = pltpu.make_async_copy(
            w_half.at[k], gathered[k].at[pl.ds(pl.multiple_of(f * rows, rows), rows)], own_sem.at[k]
        )
        copy.start()
        own.append(copy)

    for copy in b_loads:
        copy.wait()
    acc[...] = jnp.zeros_like(acc)

    def one_chunk(c, carry):
        for copy in x_loads(c):
            copy.wait()
        x = x_buf[c]
        for k in range(2):
            upper, lower = split(dot(x, basis_buf[k]))
            for q in range(per_role):
                cols = slice(q * width, (q + 1) * width)
                cot = cot_buf[k, c, :, cols]
                acc[k * per_role + q] += dot_first(upper, cot) + dot_first(lower, cot)
        return carry

    lax.fori_loop(0, CHUNKS, one_chunk, 0)
    s1 = {}
    for d in range(1, n_rep):
        s1[d] = send(
            acc.at[rep_at(d)], part_in.at[d - 1], s1_send.at[d - 1], s1_recv.at[d - 1], rep=rep_at(d)
        )
        s1[d].start()

    w2 = {}

    def forward(d):
        source = lax.rem(f - d + n_fs, n_fs)
        for k in range(2):
            w1[d, k].wait_recv()
            for e in range(1, n_rep):
                rows_ref = gathered[k].at[share_of(source, r)]
                w2[d, e, k] = send(
                    rows_ref, rows_ref, w2_send.at[d - 1, e - 1, k], w2_recv.at[d - 1, e - 1, k], rep=rep_at(e)
                )
                w2[d, e, k].start()

    forward(1)
    for k in range(2):
        upper, lower = split(dot_first(basis_buf[k], basis_buf[k]))
        gram[k, 0] = upper
        gram[k, 1] = lower

    for d in range(1, n_rep):
        s1[d].wait_recv()
    total = acc[r]
    for d in range(1, n_rep):
        total += part_in[d - 1]
    mid[...] = total.reshape(mid.shape)
    s2 = {}
    for d in range(1, n_fs):
        s2[d] = send(
            mid.at[fs_at(d)], mid_in.at[d - 1], s2_send.at[d - 1], s2_recv.at[d - 1], fs=fs_at(d)
        )
        s2[d].start()
    for d in range(2, n_fs - 1):
        forward(d)
    for d in range(1, n_fs):
        s2[d].wait_recv()
    small = mid[f]
    for d in range(1, n_fs):
        small += mid_in[d - 1]
    proj_all[r] = small

    cols = pl.ds(pl.multiple_of(lax.rem(r, per_role) * width, width), width)
    is_value = r < per_role
    first = jnp.where(is_value, value_first[:, cols], gate_first[:, cols])
    second = jnp.where(is_value, value_second[:, cols], gate_second[:, cols])
    first_new = 0.9 * first + 0.1 * small
    second_new = 0.95 * second + 0.05 * small * small
    scaled[r, f] = (first_new * lax.rsqrt(second_new)).astype(BF16)
    a4, p4, g4 = {}, {}, {}
    for d in range(1, n_fs):
        a4[d] = send(
            scaled.at[r, f], scaled.at[r, f], a_send.at[d - 1], a_recv.at[d - 1], fs=fs_at(d)
        )
        a4[d].start()
    for d in range(1, n_rep):
        p4[d] = send(proj_all.at[r], proj_all.at[r], p_send.at[d - 1], p_recv.at[d - 1], rep=rep_at(d))
        p4[d].start()
    if n_fs > 2:
        forward(n_fs - 1)
    for d in range(1, n_fs):
        a4[d].wait_recv()
    for d in range(1, n_rep):
        g4[d] = send(scaled.at[r], scaled.at[r], g_send.at[d - 1], g_recv.at[d - 1], rep=rep_at(d))
        g4[d].start()
    for d in range(1, n_rep):
        g4[d].wait_recv()

    for k in range(2):
        squares = 0.0
        for q in range(per_role):
            s = scaled[k * per_role + q].reshape(n_fs * low, width)
            squares += jnp.sum((dot(gram[k, 0], s) + dot(gram[k, 1], s)) * s.astype(F32))
        sq_buf[0, k] = jnp.full(sq_buf.shape[2:], squares, F32)
    q4 = []
    for d in range(1, n_tp):
        copy = send(
            sq_buf.at[0], sq_buf.at[d], q_send.at[d - 1], q_recv.at[d - 1], tp=lax.rem(t + d, n_tp)
        )
        copy.start()
        q4.append(copy)
    for d in range(1, n_rep):
        p4[d].wait_recv()
    scaled_out[...] = scaled[...].reshape(scaled_out.shape)
    projected_out[...] = proj_all[...]
    for copy in q4:
        copy.wait_recv()
    sums = sq_buf[0]
    for d in range(1, n_tp):
        sums += sq_buf[d]
    squares_out[...] = sums

    for copy in list(w1.values()) + list(s1.values()) + list(s2.values()) + list(a4.values()):
        copy.wait_send()
    for copy in list(p4.values()) + list(g4.values()) + q4:
        copy.wait_send()
    for copy in own:
        copy.wait()
    for copy in w2.values():
        copy.wait()


def finish(
    own_blocks, entries,
    where, value_rows, gate_rows, value_basis, gate_basis, value_weight, gate_weight,
    scaled, projected, squares, value_first, gate_first, value_second, gate_second,
    value_new, gate_new, value_copy, gate_copy, value_step, gate_step,
    value_first_new, gate_first_new, value_second_new, gate_second_new,
):
    step = pl.program_id(0)
    width = scaled.shape[2]
    per_role = scaled.shape[0] // 2
    roles = (
        (value_rows, value_basis, value_weight, value_new, value_copy, value_step),
        (gate_rows, gate_basis, gate_weight, gate_new, gate_copy, gate_step),
    )
    for k, (rows, basis, weight, new, copy, step_out) in enumerate(roles):
        factor = lax.rsqrt(squares[k, :1, :1] / entries + 1e-06)
        for q in range(per_role):
            cols = slice(q * width, (q + 1) * width)
            direction = dot(basis[...], scaled[k * per_role + q]) * factor
            copy[:, cols] = (rows[:, cols].astype(F32) - learn_rate * direction).astype(BF16)

            @pl.when(step < own_blocks)
            def _():
                step_out[:, cols] = direction
                new[:, cols] = weight[:, cols] - learn_rate * direction

    @pl.when(step == 0)
    def _():
        moments = (
            (value_first, value_second, value_first_new, value_second_new),
            (gate_first, gate_second, gate_first_new, gate_second_new),
        )
        for k, (first, second, first_new, second_new) in enumerate(moments):
            for q in range(per_role):
                cols = slice(q * width, (q + 1) * width)
                small = projected[k * per_role + q]
                first_new[:, cols] = 0.9 * first[:, cols] + 0.1 * small
                second_new[:, cols] = 0.95 * second[:, cols] + 0.05 * small * small


def local(sizes, *args):
    n_fs, n_rep, n_tp = sizes
    (mixer, value_cot, gate_cot, value_weight, gate_weight, value_basis, gate_basis,
     value_first, gate_first, value_second, gate_second) = args
    tokens, model = mixer.shape
    half = value_cot.shape[1]
    rows = value_weight.shape[0]
    rank = value_basis.shape[1]
    low = value_first.shape[0]
    width = 2 * half // n_rep
    chunk = tokens // CHUNKS
    any_spec = pl.BlockSpec(memory_space=pl.ANY)
    vmem = pl.BlockSpec(memory_space=pltpu.VMEM)
    dma = pltpu.SemaphoreType.DMA
    scratch = [
        pltpu.VMEM((CHUNKS, chunk, model), BF16),
        pltpu.VMEM((2, CHUNKS, chunk, half), BF16),
        pltpu.VMEM((2, rows, half), F32),
        pltpu.VMEM((2, rows, half), BF16),
        pltpu.VMEM((2, model, rank), BF16),
        pltpu.VMEM((2, 2, rank, rank), BF16),
        pltpu.VMEM((n_rep, rank, width), F32),
        pltpu.VMEM((n_rep - 1, rank, width), F32),
        pltpu.VMEM((n_fs, low, width), F32),
        pltpu.VMEM((n_fs - 1, low, width), F32),
        pltpu.VMEM((n_rep, low, width), F32),
        pltpu.VMEM((n_rep, n_fs, low, width), BF16),
        pltpu.VMEM((n_tp, 2, 8, 128), F32),
        dma((CHUNKS, 3)), dma((2,)), dma((2,)), dma((2,)),
        dma((n_fs - 1, 2)), dma((n_fs - 1, 2)),
        dma((n_fs - 1, n_rep - 1, 2)), dma((n_fs - 1, n_rep - 1, 2)),
    ]
    for count in (n_rep, n_fs, n_rep, n_fs, n_rep, n_tp):
        scratch += [dma((count - 1,)), dma((count - 1,))]
    value_rows, gate_rows, scaled, projected, squares = pl.pallas_call(
        functools.partial(exchange, n_fs, n_rep, n_tp),
        out_shape=(
            jax.ShapeDtypeStruct((rows * n_fs, half), BF16),
            jax.ShapeDtypeStruct((rows * n_fs, half), BF16),
            jax.ShapeDtypeStruct((n_rep, rank, width), BF16),
            jax.ShapeDtypeStruct((n_rep, low, width), F32),
            jax.ShapeDtypeStruct((2, 8, 128), F32),
        ),
        in_specs=[any_spec] * 7 + [vmem] * 4,
        out_specs=(any_spec, any_spec, vmem, vmem, vmem),
        scratch_shapes=scratch,
        compiler_params=pltpu.CompilerParams(
            collective_id=0, has_side_effects=True, vmem_limit_bytes=52 * 1024 * 1024
        ),
        name="exchange",
    )(*args)

    block = min(rows, 256)
    own_blocks = rows // block
    blocks = model // block
    where = (lax.axis_index("fs") * own_blocks).astype(jnp.int32).reshape(1)

    def turned(i, w):
        return (lax.rem(w[0] + i, blocks), 0)

    def own(i, w):
        return (jnp.minimum(i, own_blocks - 1), 0)

    def whole(shape):
        return pl.BlockSpec(shape, lambda i, w: (0,) * len(shape))

    row_spec = pl.BlockSpec((block, half), turned)
    basis_spec = pl.BlockSpec((block, rank), turned)
    own_spec = pl.BlockSpec((block, half), own)
    moment = whole((low, half))
    return pl.pallas_call(
        functools.partial(finish, own_blocks, float(model) * half * n_tp),
        grid_spec=pltpu.PrefetchScalarGridSpec(
            num_scalar_prefetch=1,
            grid=(blocks,),
            in_specs=[row_spec, row_spec, basis_spec, basis_spec, own_spec, own_spec,
                      whole(scaled.shape), whole(projected.shape), whole(squares.shape)] + [moment] * 4,
            out_specs=[own_spec, own_spec, row_spec, row_spec, own_spec, own_spec] + [moment] * 4,
        ),
        out_shape=[
            jax.ShapeDtypeStruct((rows, half), F32),
            jax.ShapeDtypeStruct((rows, half), F32),
            jax.ShapeDtypeStruct((model, half), BF16),
            jax.ShapeDtypeStruct((model, half), BF16),
            jax.ShapeDtypeStruct((rows, half), F32),
            jax.ShapeDtypeStruct((rows, half), F32),
        ] + [jax.ShapeDtypeStruct((low, half), F32)] * 4,
        compiler_params=pltpu.CompilerParams(vmem_limit_bytes=40 * 1024 * 1024),
        name="finish",
    )(where, value_rows, gate_rows, value_basis, gate_basis, value_weight, gate_weight,
      scaled, projected, squares, value_first, gate_first, value_second, gate_second)


def solution(mesh):
    sizes = tuple(mesh.shape[name] for name in ("fs", "rep", "tp"))
    return jax.shard_map(
        lambda *args: tuple(local(sizes, *args)),
        mesh=mesh,
        in_specs=(
            P(("fs", "rep"), None),
            P(("fs", "rep"), "tp"),
            P(("fs", "rep"), "tp"),
            P("fs", "tp"),
            P("fs", "tp"),
            P(),
            P(),
            P("fs", "tp"),
            P("fs", "tp"),
            P("fs", "tp"),
            P("fs", "tp"),
        ),
        out_specs=(
            P("fs", "tp"),
            P("fs", "tp"),
            P(None, "tp"),
            P(None, "tp"),
            P("fs", "tp"),
            P("fs", "tp"),
            P("fs", "tp"),
            P("fs", "tp"),
            P("fs", "tp"),
            P("fs", "tp"),
        ),
        check_vma=False,
    )
```

time: 350 us -> 159 us (0.45)
  waiting for transfers between devices: 277 us -> 0 us
  Pallas kernels: 0 us -> 151 us
  matrix products: 19.7 us -> 0 us
  blocking collectives: 15.3 us -> 0 us
  other arithmetic: 14.6 us -> 0 us
  between operations: 15.3 us -> 0.76 us
    all_gather x3 -> x0, waiting for transfers between devices: 183 us -> none  [the longest x1 81.2 us: local(): lax.all_gather(gate_new.astype(jnp.bfloat16), 'fs', axis=0, tiled=True)]
    pallas_call x0 -> x2, Pallas kernels: none -> 151 us  [the longest x1 136 us: local(): pl.pallas_call(functools.partial(exchange, n_fs, n_rep, n_tp), out_shape=...]
    psum x1 -> x0, waiting for transfers between devices: 47.5 us -> none  [local(): projected = lax.psum(partial_value, 'rep')]
    reduce_scatter x1 -> x0, waiting for transfers between devices: 46.5 us -> none  [local(): lax.psum_scatter(jnp.concatenate([value_part, gate_part], axis=1), 'fs',...]
    dot_general x8 -> x0, matrix products: 19.7 us -> none  [the longest x1 6.22 us: local(): jnp.dot(mixer_input, value_basis, preferred_element_type=jnp.float32)]
    psum x1 -> x0, blocking collectives: 15.3 us -> none  [local(): lax.psum((jnp.sum(value_full * value_full), jnp.sum(gate_full * gate_full...]
    convert_element_type x2 -> x0, other arithmetic: 10.3 us -> none  [the longest x1 5.58 us: local(): value_new.astype(jnp.bfloat16)]
    unnamed x22 -> x26, local copies, waits for them, and re-layouts: 7.86 us -> 7.22 us
  transfers between devices with their start and end apart: 5 -> 0, of which waited for: 5 -> 0; matrix products, arithmetic and copies ran while one was open for 1% -> 0% of each run, Pallas kernels for 0% -> 0%
where the time goes in v1:
time: 159 us
  Pallas kernels  151 us (95%)
  local copies, waits for them, and re-layouts  7.22 us (5%)
    pallas_call x1, Pallas kernels, local(): pl.pallas_call(functools.partial(exchange, n_fs, n_rep, n_tp), out_shape=...  136 us
    pallas_call x1, Pallas kernels, local(): pl.pallas_call(functools.partial(finish, own_blocks, float(model) * half...  14.5 us
    unnamed x26, local copies, waits for them, and re-layouts  7.22 us

profile of v1, /device:TPU:0, one launch (start us, length us, event | category | flops | bytes accessed | tf_op | source)
XLA Modules:
  0.0 158.7 jit_solution(3428758207022808676)
XLA Ops:
  0.7 0.0 copy-start.5
  0.7 0.9 copy-done.5
  1.6 0.0 copy-start.7
  1.6 0.9 copy-done.7
  2.6 0.0 copy-start.9
  2.6 0.9 copy-done.9
  3.5 0.0 copy-start.11
  3.5 0.9 copy-done.11
  4.5 0.0 copy-start
  4.5 0.0 copy-start.1
  4.5 0.0 copy-start.3
  4.5 0.0 copy-start.4
  4.5 0.0 copy-start.6
  4.5 0.0 copy-start.8
  4.5 0.0 copy-start.10
  4.5 136.3 %exchange.1 = (bf16[2048,1024]{1,0:T(8,128)(2,1)}, bf16[2048,1024]{1,0:T(8,128)(2,1)}, bf16[4,256,512]{2,1,0:T(8,128)(2,1)}, f32[4,64,512]{2,1,0:T(8,128)S(1)}, f32[2,8,128]{2,1,0:T(8,128)S(1)}) custom-call(bf16[2048,2048]{1,0:T(8,128)(2,1)} %mixer.1, bf16[2048,1024]{1,0:T(8,128)(2,1)} %value_cot.1, bf16[2048,1024]{1,0:T(8,128)(2,1)} %gate_cot.1, ...), custom_call_target="tpu_custom_call" | custom-call | tf_op jit(solution)/shard_map/exchange/pallas_call | solution.py:312
  140.8 0.0 copy-done
  140.8 0.0 copy-done.1
  140.8 0.0 copy-done.3
  140.8 0.0 copy-done.4
  140.8 0.0 copy-done.6
  140.8 0.0 copy-done.8
  140.8 0.0 copy-done.10
  140.9 0.0 copy-start.2
  140.9 2.2 %copy-done.2 = bf16[2048,1024]{1,0:T(8,128)(2,1)S(1)} copy-done((bf16[2048,1024]{1,0:T(8,128)(2,1)S(1)}, bf16[2048,1024]{1,0:T(8,128)(2,1)}, u32[]{:S(2)}) %copy-start.2) | copy-done | bytes 4194328
  143.0 0.0 copy-start.12
  143.0 1.2 copy-done.12
  144.3 14.5 %finish.1 = (f32[512,1024]{1,0:T(8,128)}, f32[512,1024]{1,0:T(8,128)}, bf16[2048,1024]{1,0:T(8,128)(2,1)}, bf16[2048,1024]{1,0:T(8,128)(2,1)}, f32[512,1024]{1,0...) custom-call(s32[1]{0:T(128)} %bitcast.where, ...), custom_call_target="tpu_custom_call" | custom-call | tf_op jit(solution)/shard_map/finish/pallas_call | solution.py:348
Async XLA Ops:
  0.7 1.0 copy-start.5
  1.6 0.9 copy-start.7
  2.6 0.9 copy-start.9
  3.5 0.9 copy-start.11
  4.5 136.3 %copy-start = (f32[512,1024]{1,0:T(8,128)S(1)}, f32[512,1024]{1,0:T(8,128)}, u32[]{:S(2)}) copy-start(f32[512,1024]{1,0:T(8,128)} %value_weight.3) | copy-start | bytes 6291460
  4.5 136.3 %copy-start.1 = (f32[512,1024]{1,0:T(8,128)S(1)}, f32[512,1024]{1,0:T(8,128)}, u32[]{:S(2)}) copy-start(f32[512,1024]{1,0:T(8,128)} %gate_weight.3) | copy-start | bytes 6291460
  4.5 136.3 %copy-start.3 = (bf16[2048,256]{1,0:T(8,128)(2,1)S(1)}, bf16[2048,256]{1,0:T(8,128)(2,1)}, u32[]{:S(2)}) copy-start(bf16[2048,256]{1,0:T(8,128)(2,1)} %value_basis.3) | copy-start | bytes 3145732
  4.5 136.4 %copy-start.4 = (bf16[2048,256]{1,0:T(8,128)(2,1)S(1)}, bf16[2048,256]{1,0:T(8,128)(2,1)}, u32[]{:S(2)}) copy-start(bf16[2048,256]{1,0:T(8,128)(2,1)} %gate_basis.3) | copy-start | bytes 3145732
  4.5 136.4 %copy-start.6 = (f32[64,1024]{1,0:T(8,128)S(1)}, f32[64,1024]{1,0:T(8,128)}, u32[]{:S(2)}) copy-start(f32[64,1024]{1,0:T(8,128)} %value_first.3) | copy-start | bytes 786436
  4.5 136.4 %copy-start.8 = (f32[64,1024]{1,0:T(8,128)S(1)}, f32[64,1024]{1,0:T(8,128)}, u32[]{:S(2)}) copy-start(f32[64,1024]{1,0:T(8,128)} %gate_first.3) | copy-start | bytes 786436
  4.5 136.4 %copy-start.10 = (f32[64,1024]{1,0:T(8,128)S(1)}, f32[64,1024]{1,0:T(8,128)}, u32[]{:S(2)}) copy-start(f32[64,1024]{1,0:T(8,128)} %value_second.3) | copy-start | bytes 786436
  140.9 2.2 %copy-start.2 = (bf16[2048,1024]{1,0:T(8,128)(2,1)S(1)}, bf16[2048,1024]{1,0:T(8,128)(2,1)}, u32[]{:S(2)}) copy-start(bf16[2048,1024]{1,0:T(8,128)(2,1)} %get-tuple-element.15.value_rows) | copy-start | bytes 12582916
  143.0 1.2 copy-start.12

commit v2 on v1

--- a/solution.py
+++ b/solution.py
@@ -29,11 +29,11 @@
 def exchange(
     n_fs, n_rep, n_tp,
     mixer, value_cot, gate_cot, value_weight, gate_weight, value_basis, gate_basis,
-    value_first, gate_first, value_second, gate_second,
+    value_first_hbm, gate_first_hbm, value_second_hbm, gate_second_hbm,
     value_rows, gate_rows, scaled_out, projected_out, squares_out,
     x_buf, cot_buf, w_buf, w_half, basis_buf, gram, acc, part_in,
-    mid, mid_in, proj_all, scaled, sq_buf,
-    x_sem, w_sem, b_sem, own_sem,
+    mid, mid_in, proj_all, scaled, sq_buf, moments,
+    x_sem, w_sem, b_sem, own_sem, m_sem,
     w1_send, w1_recv, w2_send, w2_recv,
     s1_send, s1_recv, s2_send, s2_recv, p_send, p_recv, a_send, a_recv, g_send, g_recv, q_send, q_recv,
 ):
@@ -71,11 +71,18 @@
             pltpu.make_async_copy(cots[k].at[span], cot_buf.at[k, c], x_sem.at[c, 1 + k]) for k in range(2)
         ]
 
+    m_loads = [
+        pltpu.make_async_copy(ref, moments.at[i], m_sem.at[i])
+        for i, ref in enumerate((value_first_hbm, gate_first_hbm, value_second_hbm, gate_second_hbm))
+    ]
     for copy in w_loads + b_loads:
         copy.start()
     for c in range(CHUNKS):
         for copy in x_loads(c):
             copy.start()
+
+    for copy in m_loads:
+        copy.start()
 
     barrier = pltpu.get_barrier_semaphore()
     for d in range(1, n_fs):
@@ -135,18 +142,30 @@
         )
         s1[d].start()
 
-    w2 = {}
+    w2, heard = {}, set()
+    near, far = (r + 1 - 2 * lax.rem(r, 2), lax.rem(r + 2, n_rep)) if n_rep == 4 else (None, None)
+
+    def pass_on(d, e, k, owner, peer):
+        source = lax.rem(f - d + n_fs, n_fs)
+        rows_ref = gathered[k].at[share_of(source, owner)]
+        w2[d, e, k] = send(
+            rows_ref, rows_ref, w2_send.at[d - 1, e, k], w2_recv.at[d - 1, e, k], rep=peer
+        )
+        w2[d, e, k].start()
 
     def forward(d):
-        source = lax.rem(f - d + n_fs, n_fs)
         for k in range(2):
             w1[d, k].wait_recv()
-            for e in range(1, n_rep):
-                rows_ref = gathered[k].at[share_of(source, r)]
-                w2[d, e, k] = send(
-                    rows_ref, rows_ref, w2_send.at[d - 1, e - 1, k], w2_recv.at[d - 1, e - 1, k], rep=rep_at(e)
-                )
-                w2[d, e, k].start()
+            peers = (near, far) if n_rep == 4 else [rep_at(e) for e in range(1, n_rep)]
+            for e, peer in enumerate(peers):
+                pass_on(d, e, k, r, peer)
+
+    def relay(d):
+        if n_rep == 4:
+            for e, k, owner, peer in ((0, 0, near, far), (1, 1, far, near)):
+                w2[d, e, k].wait_recv()
+                heard.add((d, e, k))
+                pass_on(d, 2, k, owner, peer)
 
     forward(1)
     for k in range(2):
@@ -168,17 +187,20 @@
         s2[d].start()
     for d in range(2, n_fs - 1):
         forward(d)
+        relay(d - 1)
     for d in range(1, n_fs):
         s2[d].wait_recv()
     small = mid[f]
     for d in range(1, n_fs):
         small += mid_in[d - 1]
-    proj_all[r] = small
+    proj_all[r] = small.astype(BF16)
 
     cols = pl.ds(pl.multiple_of(lax.rem(r, per_role) * width, width), width)
     is_value = r < per_role
-    first = jnp.where(is_value, value_first[:, cols], gate_first[:, cols])
-    second = jnp.where(is_value, value_second[:, cols], gate_second[:, cols])
+    for copy in m_loads:
+        copy.wait()
+    first = jnp.where(is_value, moments[0, :, cols], moments[1, :, cols])
+    second = jnp.where(is_value, moments[2, :, cols], moments[3, :, cols])
     first_new = 0.9 * first + 0.1 * small
     second_new = 0.95 * second + 0.05 * small * small
     scaled[r, f] = (first_new * lax.rsqrt(second_new)).astype(BF16)
@@ -193,11 +215,13 @@
         p4[d].start()
     if n_fs > 2:
         forward(n_fs - 1)
+        relay(n_fs - 2)
     for d in range(1, n_fs):
         a4[d].wait_recv()
     for d in range(1, n_rep):
         g4[d] = send(scaled.at[r], scaled.at[r], g_send.at[d - 1], g_recv.at[d - 1], rep=rep_at(d))
         g4[d].start()
+    relay(n_fs - 1)
     for d in range(1, n_rep):
         g4[d].wait_recv()
 
@@ -231,8 +255,10 @@
         copy.wait_send()
     for copy in own:
         copy.wait()
-    for copy in w2.values():
-        copy.wait()
+    for key, copy in w2.items():
+        copy.wait_send()
+        if key not in heard:
+            copy.wait_recv()
 
 
 def finish(
@@ -270,7 +296,7 @@
         for k, (first, second, first_new, second_new) in enumerate(moments):
             for q in range(per_role):
                 cols = slice(q * width, (q + 1) * width)
-                small = projected[k * per_role + q]
+                small = projected[k * per_role + q].astype(F32)
                 first_new[:, cols] = 0.9 * first[:, cols] + 0.1 * small
                 second_new[:, cols] = 0.95 * second[:, cols] + 0.05 * small * small
 
@@ -300,10 +326,11 @@
         pltpu.VMEM((n_rep - 1, rank, width), F32),
         pltpu.VMEM((n_fs, low, width), F32),
         pltpu.VMEM((n_fs - 1, low, width), F32),
-        pltpu.VMEM((n_rep, low, width), F32),
+        pltpu.VMEM((n_rep, low, width), BF16),
         pltpu.VMEM((n_rep, n_fs, low, width), BF16),
         pltpu.VMEM((n_tp, 2, 8, 128), F32),
-        dma((CHUNKS, 3)), dma((2,)), dma((2,)), dma((2,)),
+        pltpu.VMEM((4, low, half), F32),
+        dma((CHUNKS, 3)), dma((2,)), dma((2,)), dma((2,)), dma((4,)),
         dma((n_fs - 1, 2)), dma((n_fs - 1, 2)),
         dma((n_fs - 1, n_rep - 1, 2)), dma((n_fs - 1, n_rep - 1, 2)),
     ]
@@ -315,10 +342,10 @@
             jax.ShapeDtypeStruct((rows * n_fs, half), BF16),
             jax.ShapeDtypeStruct((rows * n_fs, half), BF16),
             jax.ShapeDtypeStruct((n_rep, rank, width), BF16),
-            jax.ShapeDtypeStruct((n_rep, low, width), F32),
+            jax.ShapeDtypeStruct((n_rep, low, width), BF16),
             jax.ShapeDtypeStruct((2, 8, 128), F32),
         ),
-        in_specs=[any_spec] * 7 + [vmem] * 4,
+        in_specs=[any_spec] * 11,
         out_specs=(any_spec, any_spec, vmem, vmem, vmem),
         scratch_shapes=scratch,
         compiler_params=pltpu.CompilerParams(

time: 159 us -> 138 us (0.87)
  Pallas kernels: 151 us -> 129 us
    pallas_call x1, Pallas kernels: 136 us -> 115 us  [local(): pl.pallas_call(functools.partial(exchange, n_fs, n_rep, n_tp), out_shape=...]
    unnamed x26 -> x24, local copies, waits for them, and re-layouts: 7.22 us -> 7.22 us
where the time goes in v2:
time: 138 us; the launch traced here: 137 us
  Pallas kernels  129 us (93%)
  local copies, waits for them, and re-layouts  7.22 us (5%)
    pallas_call x1, Pallas kernels, local(): pl.pallas_call(functools.partial(exchange, n_fs, n_rep, n_tp), out_shape=...  115 us
    pallas_call x1, Pallas kernels, local(): pl.pallas_call(functools.partial(finish, own_blocks, float(model) * half...  14.5 us
    unnamed x24, local copies, waits for them, and re-layouts  7.22 us

profile of v2, /device:TPU:0, one launch (start us, length us, event | category | flops | bytes accessed | tf_op | source)
XLA Modules:
  0.0 137.1 jit_solution(11721257788102966021)
XLA Ops:
  0.7 0.0 copy-start.5
  0.7 0.9 copy-done.5
  1.6 0.0 copy-start.7
  1.6 0.9 copy-done.7
  2.6 0.0 copy-start.9
  2.6 0.9 copy-done.9
  3.5 0.0 copy-start.10
  3.5 0.9 copy-done.10
  4.5 0.0 copy-start
  4.5 0.0 copy-start.1
  4.5 0.0 copy-start.3
  4.5 0.0 copy-start.4
  4.5 0.0 copy-start.6
  4.5 0.0 copy-start.8
  4.5 114.6 %exchange.1 = (bf16[2048,1024]{1,0:T(8,128)(2,1)}, bf16[2048,1024]{1,0:T(8,128)(2,1)}, bf16[4,256,512]{2,1,0:T(8,128)(2,1)}, bf16[4,64,512]{2,1,0:T(8,128)(2,1)S(1)}, f32[2,8,128]{2,1,0:T(8,128)S(1)}) custom-call(bf16[2048,2048]{1,0:T(8,128)(2,1)} %mixer.1, bf16[2048,1024]{1,0:T(8,128)(2,1)} %value_cot.1, bf16[2048,1024]{1,0:T(8,128)(2,1)} %gate_cot.1, ...), custom_call_target="tpu_custom_call" | custom-call | tf_op jit(solution)/shard_map/exchange/pallas_call | solution.py:339
  119.1 0.0 copy-done
  119.1 0.0 copy-done.1
  119.1 0.0 copy-done.3
  119.1 0.0 copy-done.4
  119.2 0.0 copy-done.6
  119.2 0.0 copy-done.8
  119.2 0.0 copy-start.2
  119.2 2.2 %copy-done.2 = bf16[2048,1024]{1,0:T(8,128)(2,1)S(1)} copy-done((bf16[2048,1024]{1,0:T(8,128)(2,1)S(1)}, bf16[2048,1024]{1,0:T(8,128)(2,1)}, u32[]{:S(2)}) %copy-start.2) | copy-done | bytes 4194328
  121.4 0.0 copy-start.11
  121.4 1.2 copy-done.11
  122.6 14.5 %finish.1 = (f32[512,1024]{1,0:T(8,128)}, f32[512,1024]{1,0:T(8,128)}, bf16[2048,1024]{1,0:T(8,128)(2,1)}, bf16[2048,1024]{1,0:T(8,128)(2,1)}, f32[512,1024]{1,0...) custom-call(s32[1]{0:T(128)} %bitcast.where, ...), custom_call_target="tpu_custom_call" | custom-call | tf_op jit(solution)/shard_map/finish/pallas_call | solution.py:375
Async XLA Ops:
  0.7 1.0 copy-start.5
  1.6 0.9 copy-start.7
  2.6 0.9 copy-start.9
  3.5 0.9 copy-start.10
  4.5 114.7 %copy-start = (f32[512,1024]{1,0:T(8,128)S(1)}, f32[512,1024]{1,0:T(8,128)}, u32[]{:S(2)}) copy-start(f32[512,1024]{1,0:T(8,128)} %value_weight.3) | copy-start | bytes 6291460
  4.5 114.7 %copy-start.1 = (f32[512,1024]{1,0:T(8,128)S(1)}, f32[512,1024]{1,0:T(8,128)}, u32[]{:S(2)}) copy-start(f32[512,1024]{1,0:T(8,128)} %gate_weight.3) | copy-start | bytes 6291460
  4.5 114.7 %copy-start.3 = (bf16[2048,256]{1,0:T(8,128)(2,1)S(1)}, bf16[2048,256]{1,0:T(8,128)(2,1)}, u32[]{:S(2)}) copy-start(bf16[2048,256]{1,0:T(8,128)(2,1)} %value_basis.3) | copy-start | bytes 3145732
  4.5 114.7 %copy-start.4 = (bf16[2048,256]{1,0:T(8,128)(2,1)S(1)}, bf16[2048,256]{1,0:T(8,128)(2,1)}, u32[]{:S(2)}) copy-start(bf16[2048,256]{1,0:T(8,128)(2,1)} %gate_basis.3) | copy-start | bytes 3145732
  4.5 114.7 %copy-start.6 = (f32[64,1024]{1,0:T(8,128)S(1)}, f32[64,1024]{1,0:T(8,128)}, u32[]{:S(2)}) copy-start(f32[64,1024]{1,0:T(8,128)} %value_first.1) | copy-start | bytes 786436
  4.5 114.7 %copy-start.8 = (f32[64,1024]{1,0:T(8,128)S(1)}, f32[64,1024]{1,0:T(8,128)}, u32[]{:S(2)}) copy-start(f32[64,1024]{1,0:T(8,128)} %gate_first.1) | copy-start | bytes 786436
  119.2 2.2 %copy-start.2 = (bf16[2048,1024]{1,0:T(8,128)(2,1)S(1)}, bf16[2048,1024]{1,0:T(8,128)(2,1)}, u32[]{:S(2)}) copy-start(bf16[2048,1024]{1,0:T(8,128)(2,1)} %get-tuple-element.15.value_rows) | copy-start | bytes 12582916
  121.4 1.2 copy-start.11
